TPU v7x, 32 devices: a whole 2x2x4 slice. The times are simulated.
32 devices in a mesh: sp: 16 (over z, y, x), tp: 2 (over core).
Axes of the slice: x: 2, y: 2, z: 4, core: 2. Of those that a mesh axis runs over, the one named last changes fastest.
Arguments:
- conv_out: bfloat16 [2048, 2048], P('sp', 'tp'), may hold values from -1500 to 1500
- ln_gain: float32 [2048], P('tp'), may hold values from 0.1 to 1.9
- taps: bfloat16 [31, 2048], P(None, 'tp'), may hold values from -1 to 1
- proj_weight: bfloat16 [2048, 2048], P('sp', 'tp'), may hold values from -0.125 to 0.125
- stream_mid: bfloat16 [2048, 2048], P('sp', 'tp'), may hold values from -6 to 6
- out_grad: bfloat16 [2048, 2048], P('sp', 'tp'), may hold values from -6 to 6
- routes: int32 [2048, 2], P('sp'), may hold values from 0 to 7, all different within a row; in each aligned block of 128 rows (0 to 127, 128 to 255, ...) at most 48 rows name the same one
- route_probs: float32 [2048, 2], P('sp'), may hold values from 0.2 to 1
- gate_slabs: bfloat16 [16, 2048, 1792], P('sp', None, 'tp'), may hold values from -0.125 to 0.125
- up_slabs: bfloat16 [16, 2048, 1792], P('sp', None, 'tp'), may hold values from -0.125 to 0.125
- down_slabs: bfloat16 [16, 1792, 2048], P('sp', 'tp'), may hold values from -0.09375 to 0.09375
Outputs:
- grad_input: bfloat16 [2048, 2048], P('sp', 'tp')
- grad_proj: float32 [2048, 2048], P('sp', 'tp')
- grad_gate: bfloat16 [16, 2048, 1792], P('sp', None, 'tp')
- grad_up: bfloat16 [16, 2048, 1792], P('sp', None, 'tp')
- grad_down: bfloat16 [16, 1792, 2048], P('sp', 'tp')
Inputs may be any that keep to these rules, and one draw needn't show every extreme that they name: `routes`: each row names two different experts. Among the rows of one device no expert is named more than 48 times, and in every draw some device's rows name some expert exactly 48 times.
All inputs are finite; a program needn't handle non-finite values.
Results may differ from a plain program's by a relative error of at most 0.015.
Values may be sent and summed in bfloat16 or wider, within the bound.
A program may use at most 128 MiB of HBM per device.

v0:
```python
import functools

import jax
import jax.numpy as jnp
from jax import lax
from jax.experimental import pallas as pl
from jax.experimental.pallas import tpu as pltpu
from jax.sharding import PartitionSpec as P

MESH = pl.DeviceIdType.MESH
F32 = jnp.float32
BF16 = jnp.bfloat16
EPS = 1e-06


def flipped(index, mask):
    bit, result = 1, index
    while bit <= mask:
        if mask & bit:
            result = result + bit * (1 - 2 * lax.rem(lax.div(index, bit), 2))
        bit *= 2
    return result


def contract(left, right, left_dim, right_dim, precision=None):
    return lax.dot_general(
        left,
        right,
        (((left_dim,), (right_dim,)), ((), ())),
        preferred_element_type=F32,
        precision=precision,
    )


def identity(size, kind):
    across = lax.broadcasted_iota(jnp.int32, (size, size), 0)
    along = lax.broadcasted_iota(jnp.int32, (size, size), 1)
    return (across == along).astype(F32).astype(kind)


def layer_kernel(
    n,
    q,
    conv_ref,
    gain_ref,
    taps_ref,
    proj_ref,
    mid_ref,
    grad_ref,
    routes_ref,
    probs_ref,
    gate_hbm,
    up_hbm,
    down_hbm,
    out_input,
    out_proj,
    out_gate,
    out_up,
    out_down,
    w_gate,
    w_up,
    w_down,
    table,
    pack,
    rows,
    prob_pack,
    prob_all,
    before_ref,
    named_ref,
    weight_ref,
    g_ref,
    u_ref,
    h_ref,
    scaled_ref,
    dg_ref,
    du_ref,
    give,
    taken,
    half,
    pair_in,
    pair_sum,
    final,
    stage_up,
    stage_down,
    stat_out,
    stat_in,
    mean_ref,
    inv_ref,
    act_all,
    w_all,
    gs_own,
    gs_all,
    p_out,
    p_in,
    p_own,
    q_sum,
    q_out,
    q_in,
    gn_ref,
    stat2_out,
    stat2_in,
    ext_ref,
    ext_f32,
    taps_f32,
    load_sem,
    send_sem,
    recv_sem,
    pass_send,
    core_send,
    core_recv,
    prob_send,
    prob_recv,
    stat_sem,
    w_send,
    w_recv,
    act_send,
    act_recv,
    give_send,
    give_recv,
    pair_send,
    pair_recv,
    fin_send,
    fin_recv,
    gs_send,
    gs_recv,
    p_send,
    p_recv,
    q_send,
    q_recv,
    halo_sem,
    out_sem,
    local_sem,
):
    me, core = lax.axis_index("sp"), lax.axis_index("tp")
    other = 1 - core
    tok, width = mid_ref.shape
    experts, _, cap, _ = pack.shape
    depth = 2 * width
    nz = n // q
    own_rows = proj_ref.shape[0]
    mine = pl.ds(pl.multiple_of(core * width, 128), width)
    my_e, parity = lax.div(me, 2), lax.rem(me, 2)
    beside = flipped(me, 1)
    my_z, my_b = lax.div(me, q), lax.rem(me, q)

    def remote(src, dst, send, recv, where):
        return pltpu.make_async_remote_copy(
            src_ref=src,
            dst_ref=dst,
            send_sem=send,
            recv_sem=recv,
            device_id=where,
            device_id_type=MESH,
        )

    def in_square(step):
        return my_z * q + lax.rem(my_b + step, q)

    def in_line(step):
        return lax.rem(my_z + step, nz) * q + my_b

    loads = [
        pltpu.make_async_copy(source.at[0], held, load_sem.at[i])
        for i, (source, held) in enumerate(
            ((gate_hbm, w_gate), (up_hbm, w_up), (down_hbm, w_down))
        )
    ]
    for copy in loads:
        copy.start()

    barrier = pltpu.get_barrier_semaphore()
    for step in range(1, n):
        pl.semaphore_signal(
            barrier, inc=1, device_id=(lax.rem(me + step, n), core), device_id_type=MESH
        )
    for step in range(q):
        pl.semaphore_signal(
            barrier, inc=1, device_id=(in_square(step), other), device_id_type=MESH
        )

    eye_f32 = identity(tok, F32)
    route_rows = contract(
        routes_ref[...].astype(F32), eye_f32, 0, 0, lax.Precision.HIGHEST
    )
    first, second = route_rows[0:1, :], route_rows[1:2, :]
    labels = lax.broadcasted_iota(jnp.int32, (experts, tok), 0).astype(F32)
    named = ((labels == first) | (labels == second)).astype(F32)
    upper = (
        lax.broadcasted_iota(jnp.int32, (tok, tok), 0)
        < lax.broadcasted_iota(jnp.int32, (tok, tok), 1)
    ).astype(F32)
    before = jnp.dot(named.astype(BF16), upper.astype(BF16), preferred_element_type=F32)
    slot = lax.broadcasted_iota(jnp.int32, (cap, tok), 0).astype(F32)
    for e in range(experts):
        hit = (slot == before[e : e + 1, :]) & (named[e : e + 1, :] > 0.5)
        table[e] = hit.astype(F32).astype(BF16)
    before_ref[...] = before
    named_ref[...] = named
    flat_table = table[...].reshape(experts * cap, tok)
    for kind, source in enumerate((mid_ref, grad_ref)):
        filled = jnp.dot(flat_table, source[...], preferred_element_type=F32)
        pack[:, kind] = filled.astype(BF16).reshape(experts, cap, width)

    pl.semaphore_wait(barrier, n - 1 + q)

    def direct(step):
        target = flipped(me, step)
        return remote(
            pack.at[lax.div(target, 2)],
            rows.at[me, :, :, mine],
            send_sem.at[step // 2],
            recv_sem.at[me],
            (target, core),
        )

    def to_side(origin, source, index):
        return remote(
            source,
            rows.at[origin, :, :, mine],
            pass_send.at[index],
            recv_sem.at[origin],
            (beside, core),
        )

    def to_core(origin, source, index):
        return remote(
            source,
            rows.at[origin, :, :, mine],
            core_send.at[index],
            core_recv.at[origin],
            (me, other),
        )

    sent = [direct(step) for step in range(2, n, 2)]
    own_side = to_side(me, pack.at[my_e], 0)
    own_core = to_core(me, pack.at[my_e], 0)
    own_side.start()
    for copy in sent:
        copy.start()
    own_core.start()
    sent += [own_side, own_core]
    own_copy = pltpu.make_async_copy(pack.at[my_e], rows.at[me, :, :, mine], local_sem.at[0])
    own_copy.start()

    prob_rows = contract(probs_ref[...], eye_f32, 0, 0, lax.Precision.HIGHEST)
    slot_wide = lax.broadcasted_iota(jnp.int32, (128, tok), 0).astype(F32)

    def prob_step(e, carry):
        chosen = jnp.where(first == e.astype(F32), prob_rows[0:1, :], prob_rows[1:2, :])
        hit = (slot_wide == before_ref[pl.ds(e, 1), :]) & (named_ref[pl.ds(e, 1), :] > 0.5)
        prob_pack[e] = contract(
            jnp.broadcast_to(chosen, (8, tok)),
            hit.astype(F32),
            1,
            1,
            lax.Precision.HIGHEST,
        )
        return carry

    lax.fori_loop(0, experts, prob_step, 0)
    prob_all[me] = prob_pack[my_e]

    chunk = 16

    def stat_step(i, carry):
        at = pl.ds(pl.multiple_of(i * chunk, chunk), chunk)
        values = conv_ref[at, :].astype(F32)
        total = jnp.sum(values, axis=1, keepdims=True)
        squares = jnp.sum(values * values, axis=1, keepdims=True)
        stat_out[0, at, :] = jnp.broadcast_to(total, (chunk, 128))
        stat_out[1, at, :] = jnp.broadcast_to(squares, (chunk, 128))
        return carry

    lax.fori_loop(0, tok // chunk, stat_step, 0)
    stat_copy = remote(stat_out, stat_in, stat_sem.at[0], stat_sem.at[1], (me, other))
    stat_copy.start()
    for step in range(1, n):
        target = flipped(me, step)
        copy = remote(
            prob_pack.at[lax.div(target, 2)],
            prob_all.at[me],
            prob_send.at[step],
            prob_recv.at[me],
            (target, core),
        )
        copy.start()
        sent.append(copy)
    stat_copy.wait()

    def normed_of(at):
        values = conv_ref[at, :].astype(F32)
        return (values - mean_ref[at, 0:1]) * inv_ref[at, 0:1]

    def act_step(i, carry):
        at = pl.ds(pl.multiple_of(i * chunk, chunk), chunk)
        mean = (stat_out[0, at, :] + stat_in[0, at, :]) / depth
        var = (stat_out[1, at, :] + stat_in[1, at, :]) / depth - mean * mean
        mean_ref[at, :] = mean
        inv_ref[at, :] = lax.rsqrt(var + EPS)
        z = normed_of(at) * gain_ref[...]
        act_all[my_b, at, :] = (z * jax.nn.sigmoid(z)).astype(BF16)
        return carry

    lax.fori_loop(0, tok // chunk, act_step, 0)
    w_all[my_z] = proj_ref[...]
    taps_f32[0 : taps_ref.shape[0], :] = taps_ref[...].astype(F32)

    for step in range(2, n + 1, 2):
        if step < n:
            origin = flipped(me, step)
            remote(
                pack.at[0], rows.at[origin, :, :, mine], send_sem.at[0], recv_sem.at[origin], (beside, core)
            ).wait_recv()
            for copy in (
                to_side(origin, rows.at[origin, :, :, mine], step // 2),
                to_core(origin, rows.at[origin, :, :, mine], step),
            ):
                copy.start()
                sent.append(copy)
        origin = flipped(me, step - 1)
        remote(
            pack.at[0], rows.at[origin, :, :, mine], send_sem.at[0], recv_sem.at[origin], (beside, core)
        ).wait_recv()
        copy = to_core(origin, rows.at[origin, :, :, mine], step - 1)
        copy.start()
        sent.append(copy)

    for step in range(1, nz):
        copy = remote(
            proj_ref, w_all.at[my_z], w_send.at[step], w_recv.at[my_z], (in_line(step), core)
        )
        copy.start()
        sent.append(copy)
    for step in range(1, q):
        copy = remote(
            act_all.at[my_b],
            act_all.at[my_b],
            act_send.at[step],
            act_recv.at[my_b],
            (in_square(step), core),
        )
        copy.start()
        sent.append(copy)

    for step in range(1, n):
        origin = flipped(me, step)
        remote(
            prob_pack.at[0], prob_all.at[origin], prob_send.at[0], prob_recv.at[origin], (beside, core)
        ).wait_recv()
    columns = contract(prob_all[:, 0, :], identity(n, F32), 0, 0, lax.Precision.HIGHEST)
    for origin in range(n):
        weight_ref[origin] = jnp.broadcast_to(columns[0:cap, origin : origin + 1], (cap, 128))

    own_copy.wait()
    theirs = pl.ds(pl.multiple_of(other * width, 128), width)
    for step in range(n):
        origin = flipped(me, step)
        remote(
            pack.at[0], rows.at[origin, :, :, theirs], core_send.at[0], core_recv.at[origin], (me, other)
        ).wait_recv()
    for copy in loads:
        copy.wait()

    tiles = 2
    blocks = n // tiles
    tile_rows = blocks * cap
    hidden = w_gate.shape[1]

    def give_copy(tile):
        return remote(
            give.at[tile], taken.at[tile], give_send.at[tile], give_recv.at[tile], (me, other)
        )

    def expert_step(tile, carry):
        base = tile * blocks
        here = rows[pl.ds(base, blocks), 0].reshape(tile_rows, depth)
        g_ref[...] = jnp.dot(here, w_gate[...], preferred_element_type=F32)
        u_ref[...] = jnp.dot(here, w_up[...], preferred_element_type=F32)
        cotangent = rows[pl.ds(base, blocks), 1].reshape(tile_rows, depth)
        h_ref[...] = contract(cotangent, w_down[...], 1, 1)

        def pointwise(i, carry):
            at = pl.ds(pl.multiple_of(i * chunk, chunk), chunk)
            to = pl.ds(pl.multiple_of(tile * tile_rows + i * chunk, chunk), chunk)
            weight = weight_ref.reshape(n * cap, 128)[to, :]
            for lane in range(0, hidden, 128):
                lanes = slice(lane, lane + 128)
                gate, up = g_ref[at, lanes], u_ref[at, lanes]
                sig = jax.nn.sigmoid(gate)
                silu = gate * sig
                scaled_ref[to, lanes] = (weight * (silu * up)).astype(BF16)
                down = weight * h_ref[at, lanes]
                dg_ref[to, lanes] = (down * up * sig * (1.0 + gate * (1.0 - sig))).astype(BF16)
                du_ref[to, lanes] = (down * silu).astype(BF16)
            return carry

        lax.fori_loop(0, tile_rows // chunk, pointwise, 0)
        span = pl.ds(pl.multiple_of(tile * tile_rows, chunk), tile_rows)

        def back(which):
            part = pl.ds(pl.multiple_of(which * width, 128), width)
            return contract(dg_ref[span, :], w_gate[part, :], 1, 1) + contract(
                du_ref[span, :], w_up[part, :], 1, 1
            )

        give[tile] = back(other).astype(BF16).reshape(blocks, cap, width)
        give_copy(tile).start()
        half[pl.ds(base, blocks)] = back(core).astype(BF16).reshape(blocks, cap, width)
        return carry

    lax.fori_loop(0, tiles, expert_step, 0)

    def add_step(tile, carry):
        give_copy(tile).wait()
        at = pl.ds(tile * blocks, blocks)
        half[at] = (half[at].astype(F32) + taken[tile].astype(F32)).astype(BF16)
        return carry

    lax.fori_loop(0, tiles, add_step, 0)

    for step in range(n - 1, 0, -2):
        origin = flipped(me, step)
        index = lax.div(origin, 2)
        copy = remote(
            half.at[origin], pair_in.at[index], pair_send.at[index], pair_recv.at[index], (beside, core)
        )
        copy.start()
        sent.append(copy)

    span_up = stage_up.shape[2]
    steps_up = depth // span_up

    def up_copies(step, slot):
        at = pl.ds(pl.multiple_of(step * span_up, span_up), span_up)
        return (
            pltpu.make_async_copy(stage_up.at[slot, 0], out_gate.at[0, at, :], out_sem.at[0, slot]),
            pltpu.make_async_copy(stage_up.at[slot, 1], out_up.at[0, at, :], out_sem.at[1, slot]),
        )

    def up_step(step, carry):
        slot = lax.rem(step, 2)

        @pl.when(step >= 2)
        def _():
            for copy in up_copies(step - 2, slot):
                copy.wait()

        at = pl.ds(pl.multiple_of(step * span_up, 128), span_up)
        left = rows[:, 0, :, at].reshape(n * cap, span_up)
        stage_up[slot, 0] = contract(left, dg_ref[...], 0, 0).astype(BF16)
        stage_up[slot, 1] = contract(left, du_ref[...], 0, 0).astype(BF16)
        for copy in up_copies(step, slot):
            copy.start()
        return carry

    span_down = stage_down.shape[2]
    steps_down = depth // span_down

    def down_copy(step, slot):
        at = pl.ds(pl.multiple_of(step * span_down, span_down), span_down)
        return pltpu.make_async_copy(stage_down.at[slot], out_down.at[0, :, at], out_sem.at[2, slot])

    def down_step(step, carry):
        slot = lax.rem(step, 2)

        @pl.when(step >= 2)
        def _():
            down_copy(step - 2, slot).wait()

        at = pl.ds(pl.multiple_of(step * span_down, 128), span_down)
        right = rows[:, 1, :, at].reshape(n * cap, span_down)
        stage_down[slot] = contract(scaled_ref[...], right, 0, 0).astype(BF16)
        down_copy(step, slot).start()
        return carry

    def pair_step(step):
        origin = flipped(me, step)
        index = lax.div(origin, 2)
        remote(
            half.at[0], pair_in.at[index], pair_send.at[0], pair_recv.at[index], (beside, core)
        ).wait_recv()
        total = (half[origin].astype(F32) + pair_in[index].astype(F32)).astype(BF16)
        if step == 0:
            final[my_e] = total
        else:
            pair_sum[index] = total
            copy = remote(
                pair_sum.at[index], final.at[my_e], fin_send.at[index], fin_recv.at[my_e], (origin, core)
            )
            copy.start()
            sent.append(copy)

    pair_steps = list(range(n - 2, -1, -2))
    for i, step in enumerate(pair_steps):
        pair_step(step)
    lax.fori_loop(0, steps_up, up_step, 0)
    lax.fori_loop(0, steps_down, down_step, 0)
    for step in range(2, n, 2):
        index = lax.div(flipped(me, step), 2)
        remote(
            pair_sum.at[0], final.at[index], fin_send.at[0], fin_recv.at[index], (beside, core)
        ).wait_recv()

    gs_total = contract(final[...].reshape(experts * cap, width), flat_table, 0, 0)
    gs_total = gs_total + contract(grad_ref[...], identity(tok, BF16), 0, 0)
    gs_own[...] = gs_total.astype(BF16).reshape(gs_own.shape)

    part = pl.ds(core * (nz // 2), nz // 2)
    for step in range(q):
        peer = lax.rem(my_b + step, q)
        for flip in range(2):
            if step == 0 and flip == 0:
                continue
            copy = remote(
                gs_own.at[:, peer],
                gs_all.at[my_b, part],
                gs_send.at[step, flip],
                gs_recv.at[my_b, core],
                (my_z * q + peer, other if flip else core),
            )
            copy.start()
            sent.append(copy)
    gs_copy = pltpu.make_async_copy(gs_own.at[:, my_b], gs_all.at[my_b, part], local_sem.at[1])
    gs_copy.start()
    for step in range(1, nz):
        origin = lax.rem(my_z + step, nz)
        remote(
            proj_ref, w_all.at[origin], w_send.at[0], w_recv.at[origin], (beside, core)
        ).wait_recv()
    for step in range(1, q):
        origin = lax.rem(my_b + step, q)
        remote(
            act_all.at[origin], act_all.at[origin], act_send.at[0], act_recv.at[origin], (beside, core)
        ).wait_recv()
    gs_copy.wait()
    for step in range(q):
        origin = lax.rem(my_b + step, q)
        for flip in range(2):
            if step == 0 and flip == 0:
                continue
            source = other if flip else core
            remote(
                gs_own.at[:, 0],
                gs_all.at[origin, pl.ds(source * (nz // 2), nz // 2)],
                gs_send.at[0, 0],
                gs_recv.at[origin, source],
                (me, other),
            ).wait_recv()

    line_rows = nz * own_rows
    for b in range(q):
        product = jnp.dot(
            gs_all[b].reshape(line_rows, tok), act_all[b], preferred_element_type=F32
        ).reshape(nz, own_rows, width)
        q_sum[...] = product if b == 0 else q_sum[...] + product
    q_out[...] = q_sum[...].astype(BF16)
    for step in range(1, nz):
        target = lax.rem(my_z + step, nz)
        copy = remote(
            q_out.at[target], q_in.at[my_z], q_send.at[step], q_recv.at[my_z], (in_line(step), core)
        )
        copy.start()
        sent.append(copy)

    w_line = w_all[...].reshape(line_rows, width)
    for step in range(1, q):
        target = lax.rem(my_b + step, q)
        p_out[target] = contract(gs_all[target].reshape(line_rows, tok), w_line, 0, 0).astype(BF16)
        copy = remote(
            p_out.at[target], p_in.at[my_b], p_send.at[step], p_recv.at[my_b], (in_square(step), core)
        )
        copy.start()
        sent.append(copy)
    p_own[...] = contract(gs_all[my_b].reshape(line_rows, tok), w_line, 0, 0)
    for step in range(1, q):
        origin = lax.rem(my_b + step, q)
        remote(
            p_out.at[0], p_in.at[origin], p_send.at[0], p_recv.at[origin], (beside, core)
        ).wait_recv()

    def gn_step(i, carry):
        at = pl.ds(pl.multiple_of(i * chunk, chunk), chunk)
        grad_act = p_own[at, :]
        for step in range(1, q):
            grad_act = grad_act + p_in[lax.rem(my_b + step, q), at, :].astype(F32)
        normed = normed_of(at)
        z = normed * gain_ref[...]
        sig = jax.nn.sigmoid(z)
        gn = grad_act * sig * (1.0 + z * (1.0 - sig)) * gain_ref[...]
        gn_ref[at, :] = gn
        stat2_out[0, at, :] = jnp.broadcast_to(jnp.sum(gn, axis=1, keepdims=True), (chunk, 128))
        stat2_out[1, at, :] = jnp.broadcast_to(
            jnp.sum(gn * normed, axis=1, keepdims=True), (chunk, 128)
        )
        return carry

    lax.fori_loop(0, tok // chunk, gn_step, 0)
    stat2_copy = remote(stat2_out, stat2_in, stat_sem.at[2], stat_sem.at[3], (me, other))
    stat2_copy.start()
    stat2_copy.wait()

    def conv_grad_step(i, carry):
        at = pl.ds(pl.multiple_of(i * chunk, chunk), chunk)
        first_mean = (stat2_out[0, at, :] + stat2_in[0, at, :])[:, 0:1] / depth
        second_mean = (stat2_out[1, at, :] + stat2_in[1, at, :])[:, 0:1] / depth
        grad_conv = inv_ref[at, 0:1] * (gn_ref[at, :] - first_mean - normed_of(at) * second_mean)
        ext_ref[at, :] = grad_conv.astype(BF16)
        return carry

    lax.fori_loop(0, tok // chunk, conv_grad_step, 0)

    reach = ext_ref.shape[0] - tok
    previous = lax.rem(me + n - 1, n)
    halo = remote(
        ext_ref.at[pl.ds(0, reach)],
        ext_ref.at[pl.ds(tok, reach)],
        halo_sem.at[0],
        halo_sem.at[1],
        (previous, core),
    )
    halo.start()
    ext_f32[0:tok, :] = ext_ref[0:tok, :].astype(F32)
    halo.wait()
    after = ext_ref[tok : tok + reach, :].astype(F32)
    ext_f32[tok : tok + reach, :] = jnp.where(me == n - 1, 0.0, after)

    def conv_step(i, carry):
        lanes = pl.ds(pl.multiple_of(i * 128, 128), 128)
        total = jnp.zeros((tok, 128), F32)
        for k in range(taps_ref.shape[0]):
            total = total + taps_f32[k : k + 1, lanes] * ext_f32[k : k + tok, lanes]
        out_input[:, lanes] = total.astype(BF16)
        return carry

    lax.fori_loop(0, width // 128, conv_step, 0)

    for step in range(1, nz):
        origin = lax.rem(my_z + step, nz)
        remote(
            q_out.at[0], q_in.at[origin], q_send.at[0], q_recv.at[origin], (beside, core)
        ).wait_recv()
    proj_total = q_sum[my_z]
    for step in range(1, nz):
        proj_total = proj_total + q_in[lax.rem(my_z + step, nz)].astype(F32)
    out_proj[...] = proj_total

    for step in range(steps_up - 2, steps_up):
        for copy in up_copies(step, step % 2):
            copy.wait()
    for step in range(steps_down - 2, steps_down):
        down_copy(step, step % 2).wait()
    for copy in sent:
        copy.wait_send()


def on_device(
    conv_out,
    ln_gain,
    taps,
    proj_weight,
    stream_mid,
    out_grad,
    routes,
    route_probs,
    gate_slabs,
    up_slabs,
    down_slabs,
):
    n = lax.axis_size("sp")
    q = 1
    while q * q * 4 <= n:
        q *= 2
    nz = n // q
    tok, width = conv_out.shape
    experts = n // 2
    cap = -(-(3 * tok // experts) // 16) * 16
    own_rows = proj_weight.shape[0]
    hidden = gate_slabs.shape[2]
    slots = n * cap
    reach = -(-(taps.shape[0] - 1) // 16) * 16
    vmem, dma = pltpu.VMEM, pltpu.SemaphoreType.DMA
    near = pl.BlockSpec(memory_space=pltpu.VMEM)
    far = pl.BlockSpec(memory_space=pl.ANY)
    return pl.pallas_call(
        functools.partial(layer_kernel, n, q),
        out_shape=(
            jax.ShapeDtypeStruct((tok, width), BF16),
            jax.ShapeDtypeStruct((own_rows, width), F32),
            jax.ShapeDtypeStruct(gate_slabs.shape, BF16),
            jax.ShapeDtypeStruct(up_slabs.shape, BF16),
            jax.ShapeDtypeStruct(down_slabs.shape, BF16),
        ),
        in_specs=[near] * 8 + [far] * 3,
        out_specs=(near, near, far, far, far),
        scratch_shapes=[
            vmem(gate_slabs.shape[1:], BF16),
            vmem(up_slabs.shape[1:], BF16),
            vmem(down_slabs.shape[1:], BF16),
            vmem((experts, cap, tok), BF16),
            vmem((experts, 2, cap, width), BF16),
            vmem((n, 2, cap, 2 * width), BF16),
            vmem((experts, 8, 128), F32),
            vmem((n, 8, 128), F32),
            vmem((experts, tok), F32),
            vmem((experts, tok), F32),
            vmem((n, cap, 128), F32),
            vmem((slots // 2, hidden), F32),
            vmem((slots // 2, hidden), F32),
            vmem((slots // 2, hidden), F32),
            vmem((slots, hidden), BF16),
            vmem((slots, hidden), BF16),
            vmem((slots, hidden), BF16),
            vmem((2, n // 2, cap, width), BF16),
            vmem((2, n // 2, cap, width), BF16),
            vmem((n, cap, width), BF16),
            vmem((experts, cap, width), BF16),
            vmem((experts, cap, width), BF16),
            vmem((experts, cap, width), BF16),
            vmem((2, 2, 256, hidden), BF16),
            vmem((2, hidden, 512), BF16),
            vmem((2, tok, 128), F32),
            vmem((2, tok, 128), F32),
            vmem((tok, 128), F32),
            vmem((tok, 128), F32),
            vmem((q, tok, width), BF16),
            vmem((nz, own_rows, width), BF16),
            vmem((nz // 2, q, own_rows, tok), BF16),
            vmem((q, nz, own_rows, tok), BF16),
            vmem((q, tok, width), BF16),
            vmem((q, tok, width), BF16),
            vmem((tok, width), F32),
            vmem((nz, own_rows, width), F32),
            vmem((nz, own_rows, width), BF16),
            vmem((nz, own_rows, width), BF16),
            vmem((tok, width), F32),
            vmem((2, tok, 128), F32),
            vmem((2, tok, 128), F32),
            vmem((tok + reach, width), BF16),
            vmem((tok + reach, width), F32),
            vmem((-(-taps.shape[0] // 8) * 8, width), F32),
            dma((3,)),
            dma((n // 2,)),
            dma((n,)),
            dma((n // 2,)),
            dma((n,)),
            dma((n,)),
            dma((n,)),
            dma((n,)),
            dma((4,)),
            dma((nz,)),
            dma((nz,)),
            dma((q,)),
            dma((q,)),
            dma((2,)),
            dma((2,)),
            dma((experts,)),
            dma((experts,)),
            dma((experts,)),
            dma((experts,)),
            dma((q, 2)),
            dma((q, 2)),
            dma((q,)),
            dma((q,)),
            dma((nz,)),
            dma((nz,)),
            dma((2,)),
            dma((3, 2)),
            dma((2,)),
        ],
        compiler_params=pltpu.CompilerParams(
            collective_id=0, has_side_effects=True, vmem_limit_bytes=66 * 2**20 - 2**21
        ),
        cost_estimate=pl.CostEstimate(
            flops=16 * slots * 2 * width * hidden, bytes_accessed=60_000_000, transcendentals=0
        ),
    )(
        conv_out,
        ln_gain[None],
        taps,
        proj_weight,
        stream_mid,
        out_grad,
        routes,
        route_probs,
        gate_slabs,
        up_slabs,
        down_slabs,
    )


def solution(mesh):
    return jax.shard_map(
        on_device,
        mesh=mesh,
        in_specs=(
            P("sp", "tp"),
            P("tp"),
            P(None, "tp"),
            P("sp", "tp"),
            P("sp", "tp"),
            P("sp", "tp"),
            P("sp", None),
            P("sp", None),
            P("sp", None, "tp"),
            P("sp", None, "tp"),
            P("sp", "tp", None),
        ),
        out_specs=(
            P("sp", "tp"),
            P("sp", "tp"),
            P("sp", None, "tp"),
            P("sp", None, "tp"),
            P("sp", "tp", None),
        ),
        check_vma=False,
    )
```

profile of v0, /device:TPU:14, one launch (start us, length us, event | category | flops | bytes accessed | tf_op | source)
XLA Modules:
  0.0 155.7 jit_solution(2115548734509644741)
XLA Ops:
  0.6 1.4 copy.16.routes_ref
  2.0 1.4 copy.17.probs_ref
  3.5 139.1 %shard_map.146 = (bf16[128,1024]{1,0:T(8,128)(2,1)}, f32[128,1024]{1,0:T(8,128)}, bf16[1,2048,896]{2,1,0:T(8,128)(2,1)}, bf16[1,2048,896]{2,1,0:T(8,128)(2,1)}, bf16[1,896,2048]{2,1,0:T(8,128)(2,1)}) custom-call(bf16[128,1024]{1,0:T(8,128)(2,1)} %conv_ref.1, f32[1,1024]{1,0:T(1,128)} %bitcast.1, bf16[31,1024]{1,0:T(8,128)(2,1)} %taps_ref.1, ...), custom_call_target="tpu_custom_call" | custom-call | flops 22548578304 | bytes 60000000 | tf_op jit(solution)/shard_map/pallas_call | solution.py:684
  142.6 1.7 %copy.23 = bf16[128,1024]{1,0:T(8,128)(2,1)} copy(bf16[128,1024]{1,0:T(8,128)(2,1)} %get-tuple-element.10) | data formatting | bytes 524288
  144.3 1.9 %copy.24 = f32[128,1024]{1,0:T(8,128)} copy(f32[128,1024]{1,0:T(8,128)} %get-tuple-element.11) | data formatting | bytes 1048576
  146.2 0.0 copy-start.1
  146.2 4.3 %copy.25 = bf16[1,2048,896]{2,1,0:T(8,128)(2,1)} copy(bf16[1,2048,896]{2,1,0:T(8,128)(2,1)} %get-tuple-element.12) | data formatting | bytes 7340032
  150.5 0.0 copy-done.1
  150.5 0.0 copy-start
  150.5 1.9 %copy.26 = bf16[1,2048,896]{2,1,0:T(8,128)(2,1)} copy(bf16[1,2048,896]{2,1,0:T(8,128)(2,1)S(1)} %copy-done.1) | data formatting | bytes 7340032
  152.4 1.5 copy-done
  153.8 1.8 %copy.27 = bf16[1,896,2048]{2,1,0:T(8,128)(2,1)} copy(bf16[1,896,2048]{2,1,0:T(8,128)(2,1)S(1)} %copy-done) | data formatting | bytes 7340032
Async XLA Ops:
  146.2 4.3 %copy-start.1 = (bf16[1,2048,896]{2,1,0:T(8,128)(2,1)S(1)}, bf16[1,2048,896]{2,1,0:T(8,128)(2,1)}, u32[]{:S(2)}) copy-start(bf16[1,2048,896]{2,1,0:T(8,128)(2,1)} %get-tuple-element.13) | copy-start | bytes 11010052
  150.5 3.4 %copy-start = (bf16[1,896,2048]{2,1,0:T(8,128)(2,1)S(1)}, bf16[1,896,2048]{2,1,0:T(8,128)(2,1)}, u32[]{:S(2)}) copy-start(bf16[1,896,2048]{2,1,0:T(8,128)(2,1)} %get-tuple-element.14) | copy-start | bytes 11010052
where the time goes:
time: 156 us
  Pallas kernels  139 us (89%)
  local copies, waits for them, and re-layouts  15.9 us (10%)
    pallas_call x1, Pallas kernels, on_device(): pl.pallas_call(functools.partial(layer_kernel, n, q), out_shape=(jax.Shap...  139 us
    unnamed x11, local copies, waits for them, and re-layouts  15.9 us

commit v1 on v0

v1 whole, which is shorter than its diff:
```python
import functools

import jax
import jax.numpy as jnp
from jax import lax
from jax.experimental import pallas as pl
from jax.experimental.pallas import tpu as pltpu
from jax.sharding import PartitionSpec as P

MESH = pl.DeviceIdType.MESH
F32 = jnp.float32
BF16 = jnp.bfloat16
EPS = 1e-06
VMEM_BYTES = 64 * 2**20
CHUNKS = 4


def flipped(index, mask):
    bit, result = 1, index
    while bit <= mask:
        if mask & bit:
            result = result + bit * (1 - 2 * lax.rem(lax.div(index, bit), 2))
        bit *= 2
    return result


def contract(left, right, left_dim, right_dim, precision=None):
    return lax.dot_general(
        left,
        right,
        (((left_dim,), (right_dim,)), ((), ())),
        preferred_element_type=F32,
        precision=precision,
    )


def identity(size, kind):
    across = lax.broadcasted_iota(jnp.int32, (size, size), 0)
    along = lax.broadcasted_iota(jnp.int32, (size, size), 1)
    return (across == along).astype(F32).astype(kind)


def layer_kernel(
    n,
    q,
    conv_ref,
    gain_ref,
    proj_ref,
    mid_ref,
    grad_ref,
    routes_ref,
    probs_ref,
    gate_hbm,
    up_hbm,
    down_hbm,
    out_ext,
    out_proj,
    out_gate,
    out_up,
    out_down,
    w_gate,
    w_up,
    w_down,
    table,
    pack,
    rows,
    prob_pack,
    prob_all,
    before_ref,
    named_ref,
    weight_ref,
    g_ref,
    u_ref,
    h_ref,
    scaled_ref,
    dg_ref,
    du_ref,
    give,
    taken,
    half,
    pair_in,
    final,
    stage_up,
    stage_down,
    stat_out,
    stat_in,
    mean_ref,
    inv_ref,
    act_all,
    w_all,
    gs_own,
    gs_all,
    p_out,
    p_in,
    p_own,
    q_sum,
    q_out,
    q_in,
    q_near,
    gn_ref,
    ext_ref,
    load_sem,
    send_sem,
    recv_sem,
    pass_send,
    core_send,
    core_recv,
    prob_send,
    prob_recv,
    stat_sem,
    w_send,
    w_recv,
    act_send,
    act_recv,
    give_send,
    give_recv,
    pair_send,
    pair_recv,
    fin_send,
    fin_recv,
    gs_send,
    gs_recv,
    p_send,
    p_recv,
    q_send,
    q_recv,
    near_recv,
    halo_sem,
    out_sem,
    local_sem,
):
    opened = []

    def phase(name):
        if opened:
            opened.pop().__exit__(None, None, None)
        if name:
            opened.append(jax.named_scope(name))
            opened[-1].__enter__()

    me, core = lax.axis_index("sp"), lax.axis_index("tp")
    other = 1 - core
    tok, width = mid_ref.shape
    experts, _, cap, _ = pack.shape
    depth = 2 * width
    nz = n // q
    own_rows = proj_ref.shape[0]
    mine = pl.ds(pl.multiple_of(core * width, 128), width)
    my_e, parity = lax.div(me, 2), lax.rem(me, 2)
    beside = flipped(me, 1)
    my_z, my_b = lax.div(me, q), lax.rem(me, q)

    def remote(src, dst, send, recv, where):
        return pltpu.make_async_remote_copy(
            src_ref=src,
            dst_ref=dst,
            send_sem=send,
            recv_sem=recv,
            device_id=where,
            device_id_type=MESH,
        )

    def in_square(step):
        return my_z * q + lax.rem(my_b + step, q)

    def in_line(step):
        return lax.rem(my_z + step, nz) * q + my_b

    phase("a_pack")
    loads = [
        pltpu.make_async_copy(source.at[0], held, load_sem.at[i])
        for i, (source, held) in enumerate(
            ((gate_hbm, w_gate), (up_hbm, w_up), (down_hbm, w_down))
        )
    ]
    for copy in loads:
        copy.start()

    barrier = pltpu.get_barrier_semaphore()
    for step in range(1, n):
        pl.semaphore_signal(
            barrier, inc=1, device_id=(lax.rem(me + step, n), core), device_id_type=MESH
        )
    for step in range(q):
        pl.semaphore_signal(
            barrier, inc=1, device_id=(in_square(step), other), device_id_type=MESH
        )

    route_rows = routes_ref[...].astype(F32)
    first, second = route_rows[0:1, :], route_rows[1:2, :]
    labels = lax.broadcasted_iota(jnp.int32, (experts, tok), 0).astype(F32)
    named = ((labels == first) | (labels == second)).astype(F32)
    upper = (
        lax.broadcasted_iota(jnp.int32, (tok, tok), 0)
        < lax.broadcasted_iota(jnp.int32, (tok, tok), 1)
    ).astype(F32)
    before = jnp.dot(named.astype(BF16), upper.astype(BF16), preferred_element_type=F32)
    slot = lax.broadcasted_iota(jnp.int32, (cap, tok), 0).astype(F32)
    for e in range(experts):
        hit = (slot == before[e : e + 1, :]) & (named[e : e + 1, :] > 0.5)
        table[e] = hit.astype(F32).astype(BF16)
    before_ref[...] = before
    named_ref[...] = named
    flat_table = table[...].reshape(experts * cap, tok)
    for kind, source in enumerate((mid_ref, grad_ref)):
        filled = jnp.dot(flat_table, source[...], preferred_element_type=F32)
        pack[:, kind] = filled.astype(BF16).reshape(experts, cap, width)

    prob_rows = probs_ref[...]
    slot_wide = lax.broadcasted_iota(jnp.int32, (128, tok), 0).astype(F32)

    def prob_step(e, carry):
        chosen = jnp.where(first == lax.convert_element_type(e, F32), prob_rows[0:1, :], prob_rows[1:2, :])
        hit = (slot_wide == before_ref[pl.ds(e, 1), :]) & (named_ref[pl.ds(e, 1), :] > 0.5)
        prob_pack[e] = contract(
            jnp.broadcast_to(chosen, (8, tok)),
            hit.astype(F32),
            1,
            1,
            lax.Precision.HIGHEST,
        )
        return carry

    lax.fori_loop(0, experts, prob_step, 0, unroll=4)
    prob_all[me] = prob_pack[my_e]

    phase("b_barrier_send")
    pl.semaphore_wait(barrier, n - 1 + q)

    def direct(step, kind):
        target = flipped(me, step)
        return remote(
            pack.at[lax.div(target, 2), kind],
            rows.at[me, kind, :, mine],
            send_sem.at[kind, step // 2],
            recv_sem.at[kind, me],
            (target, core),
        )

    def to_side(origin, kind, source, index):
        return remote(
            source,
            rows.at[origin, kind, :, mine],
            pass_send.at[kind, index],
            recv_sem.at[kind, origin],
            (beside, core),
        )

    def to_core(origin, kind, source, index):
        return remote(
            source,
            rows.at[origin, kind, :, mine],
            core_send.at[kind, index],
            core_recv.at[kind, origin],
            (me, other),
        )

    sent = []

    def begin(copy):
        copy.start()
        sent.append(copy)

    for kind in range(2):
        begin(to_side(me, kind, pack.at[my_e, kind], 0))
    for step in range(1, n):
        target = flipped(me, step)
        begin(
            remote(
                prob_pack.at[lax.div(target, 2)],
                prob_all.at[me],
                prob_send.at[step],
                prob_recv.at[me],
                (target, core),
            )
        )
    for step in range(2, n, 2):
        for kind in range(2):
            begin(direct(step, kind))
    for kind in range(2):
        begin(to_core(me, kind, pack.at[my_e, kind], 0))
    own_copy = pltpu.make_async_copy(pack.at[my_e], rows.at[me, :, :, mine], local_sem.at[0])
    own_copy.start()

    phase("c_prob_norm")
    chunk = 16

    def stat_step(i, carry):
        at = pl.ds(pl.multiple_of(i * chunk, chunk), chunk)
        values = conv_ref[at, :].astype(F32)
        total = jnp.sum(values, axis=1, keepdims=True)
        squares = jnp.sum(values * values, axis=1, keepdims=True)
        stat_out[0, at, :] = jnp.broadcast_to(total, (chunk, 128))
        stat_out[1, at, :] = jnp.broadcast_to(squares, (chunk, 128))
        return carry

    lax.fori_loop(0, tok // chunk, stat_step, 0)
    stat_copy = remote(stat_out, stat_in, stat_sem.at[0], stat_sem.at[1], (me, other))
    stat_copy.start()
    def normed_of(at):
        values = conv_ref[at, :].astype(F32)
        return (values - mean_ref[at, 0:1]) * inv_ref[at, 0:1]

    def act_step(i, carry):
        at = pl.ds(pl.multiple_of(i * chunk, chunk), chunk)
        mean = (stat_out[0, at, :] + stat_in[0, at, :]) / depth
        var = (stat_out[1, at, :] + stat_in[1, at, :]) / depth - mean * mean
        mean_ref[at, :] = mean
        inv_ref[at, :] = lax.rsqrt(var + EPS)
        z = normed_of(at) * gain_ref[...]
        act_all[my_b, at, :] = (z * jax.nn.sigmoid(z)).astype(BF16)
        return carry

    def act_part():
        stat_copy.wait()
        lax.fori_loop(0, tok // chunk, act_step, 0)
        w_all[my_z] = proj_ref[...]
        for part in range(2, q, 2):
            begin(act_copy(my_b, part))

    def act_copy(origin, step):
        return remote(
            act_all.at[origin],
            act_all.at[origin],
            act_send.at[step, lax.rem(origin, 2)],
            act_recv.at[origin],
            (flipped(me, step), core),
        )

    def act_arrival(origin):
        remote(
            act_all.at[origin], act_all.at[origin], act_send.at[1, 0], act_recv.at[origin], (beside, core)
        ).wait_recv()

    def w_copy(origin, step):
        return remote(
            w_all.at[origin],
            w_all.at[origin],
            w_send.at[step, lax.div(origin, nz // 2)],
            w_recv.at[origin],
            (flipped(me, step * q), core),
        )

    def w_arrival(origin):
        remote(
            w_all.at[origin], w_all.at[origin], w_send.at[1, 0], w_recv.at[origin], (beside, core)
        ).wait_recv()

    def arrived(origin, kind):
        remote(
            pack.at[0, 0],
            rows.at[origin, kind, :, mine],
            send_sem.at[0, 0],
            recv_sem.at[kind, origin],
            (beside, core),
        ).wait_recv()

    def relay(step):
        phase("d_relay%02d" % step)
        origin = flipped(me, step)
        for kind in range(2):
            arrived(origin, kind)
            source = rows.at[origin, kind, :, mine]
            if step % 2 == 0:
                begin(to_side(origin, kind, source, step // 2))
            begin(to_core(origin, kind, source, step))

    tile_rows = q * cap
    hidden = w_gate.shape[1]
    theirs = pl.ds(pl.multiple_of(other * width, 128), width)

    def tile_base(tile):
        return flipped(my_z, tile) * q

    def tile_span(tile):
        return pl.ds(pl.multiple_of(tile_base(tile) * cap, chunk), tile_rows)

    def ready(tile):
        for step in range(tile * q, tile * q + q):
            origin = flipped(me, step)
            for kind in range(2):
                remote(
                    pack.at[0, 0],
                    rows.at[origin, kind, :, theirs],
                    core_send.at[0, 0],
                    core_recv.at[kind, origin],
                    (me, other),
                ).wait_recv()

    def prob_part():
        for step in range(1, n):
            origin = flipped(me, step)
            remote(
                prob_pack.at[0],
                prob_all.at[origin],
                prob_send.at[0],
                prob_recv.at[origin],
                (beside, core),
            ).wait_recv()
        columns = contract(prob_all[:, 0, :], identity(n, F32), 0, 0, lax.Precision.HIGHEST)
        for origin in range(n):
            weight_ref[origin] = jnp.broadcast_to(columns[0:cap, origin : origin + 1], (cap, 128))

    def front(tile):
        phase("g_front%d" % tile)
        ready(tile)
        at = pl.ds(tile_base(tile), q)
        here = rows[at, 0].reshape(tile_rows, depth)
        g_ref[...] = jnp.dot(here, w_gate[...], preferred_element_type=F32)
        u_ref[...] = jnp.dot(here, w_up[...], preferred_element_type=F32)
        cotangent = rows[at, 1].reshape(tile_rows, depth)
        h_ref[...] = contract(cotangent, w_down[...], 1, 1)
        first_row = tile_base(tile) * cap

        def pointwise(i, carry):
            at = pl.ds(pl.multiple_of(i * chunk, chunk), chunk)
            to = pl.ds(pl.multiple_of(first_row + i * chunk, chunk), chunk)
            weight = weight_ref.reshape(n * cap, 128)[to, :]
            for lane in range(0, hidden, 128):
                lanes = slice(lane, lane + 128)
                gate, up = g_ref[at, lanes], u_ref[at, lanes]
                sig = jax.nn.sigmoid(gate)
                silu = gate * sig
                scaled_ref[to, lanes] = (weight * (silu * up)).astype(BF16)
                down = weight * h_ref[at, lanes]
                dg_ref[to, lanes] = (down * up * sig * (1.0 + gate * (1.0 - sig))).astype(BF16)
                du_ref[to, lanes] = (down * silu).astype(BF16)
            return carry

        lax.fori_loop(0, tile_rows // chunk, pointwise, 0)

    def back(tile):
        phase("h_back%d" % tile)
        span = tile_span(tile)

        def product(which):
            part = pl.ds(pl.multiple_of(which * width, 128), width)
            total = contract(dg_ref[span, :], w_gate[part, :], 1, 1)
            total = total + contract(du_ref[span, :], w_up[part, :], 1, 1)
            return total.astype(BF16).reshape(q, cap, width)

        give[tile] = product(other)
        copy = remote(
            give.at[tile], taken.at[tile], give_send.at[tile], give_recv.at[tile], (me, other)
        )
        copy.start()
        kept = product(core)
        copy.wait()
        total = kept.astype(F32) + taken[tile].astype(F32)
        half[pl.ds(tile_base(tile), q)] = total.astype(BF16)

    def pair_send_tile(tile):
        for step in range(tile * q + 1, tile * q + q, 2):
            origin = flipped(me, step)
            index = lax.div(origin, 2)
            begin(
                remote(
                    half.at[origin],
                    pair_in.at[index],
                    pair_send.at[index],
                    pair_recv.at[index],
                    (beside, core),
                )
            )

    def pair_sum_tile(tile):
        phase("i_pair%d" % tile)
        for step in range(tile * q, tile * q + q, 2):
            origin = flipped(me, step)
            index = lax.div(origin, 2)
            remote(
                half.at[0], pair_in.at[index], pair_send.at[0], pair_recv.at[index], (beside, core)
            ).wait_recv()
            total = (half[origin].astype(F32) + pair_in[index].astype(F32)).astype(BF16)
            if step == 0:
                final[my_e] = total
            else:
                half[origin] = total
                begin(
                    remote(
                        half.at[origin],
                        final.at[my_e],
                        fin_send.at[index],
                        fin_recv.at[my_e],
                        (origin, core),
                    )
                )

    span_up = stage_up.shape[2]
    steps_up = depth // span_up

    def up_copies(step, slot):
        at = pl.ds(pl.multiple_of(step * span_up, span_up), span_up)
        return (
            pltpu.make_async_copy(stage_up.at[slot, 0], out_gate.at[0, at, :], out_sem.at[0, slot]),
            pltpu.make_async_copy(stage_up.at[slot, 1], out_up.at[0, at, :], out_sem.at[1, slot]),
        )

    def up_step(step, carry):
        slot = lax.rem(step, 2)

        @pl.when(step >= 2)
        def _():
            for copy in up_copies(step - 2, slot):
                copy.wait()

        at = pl.ds(pl.multiple_of(step * span_up, 128), span_up)
        left = rows[:, 0, :, at].reshape(n * cap, span_up)
        stage_up[slot, 0] = contract(left, dg_ref[...], 0, 0).astype(BF16)
        stage_up[slot, 1] = contract(left, du_ref[...], 0, 0).astype(BF16)
        for copy in up_copies(step, slot):
            copy.start()
        return carry

    span_down = stage_down.shape[2]
    steps_down = depth // span_down

    def down_copy(step, slot):
        at = pl.ds(pl.multiple_of(step * span_down, span_down), span_down)
        return pltpu.make_async_copy(stage_down.at[slot], out_down.at[0, :, at], out_sem.at[2, slot])

    def down_step(step, carry):
        slot = lax.rem(step, 2)

        @pl.when(step >= 2)
        def _():
            down_copy(step - 2, slot).wait()

        at = pl.ds(pl.multiple_of(step * span_down, 128), span_down)
        right = rows[:, 1, :, at].reshape(n * cap, span_down)
        stage_down[slot] = contract(scaled_ref[...], right, 0, 0).astype(BF16)
        down_copy(step, slot).start()
        return carry

    far_tile, last_tile = nz - 2, nz - 1
    near_tiles = list(range(nz - 2))

    def start_gathers():
        for part in range(1, nz // 2 + 1):
            begin(w_copy(my_z, part))

    work = {}

    def after(step, *actions):
        work.setdefault(min(step, n - 1), []).extend(actions)

    def before_tiles():
        phase("f_prob")
        prob_part()
        own_copy.wait()
        for copy in loads:
            copy.wait()

    after(1, act_part)
    after(2 * q, before_tiles)
    for tile in near_tiles:
        after(max((tile + 1) * q + 2, 2 * q), functools.partial(front, tile))
    for tile in near_tiles[:-1]:
        after(n - q, functools.partial(back, tile))
    after(n - 2, start_gathers, functools.partial(front, far_tile))
    after(n - 3, functools.partial(back, far_tile), functools.partial(pair_send_tile, far_tile))
    for tile in near_tiles[:-1]:
        after(n - 3, functools.partial(pair_send_tile, tile))

    order = []
    for step in range(2, n, 2):
        order += [step, step - 1]
    for step in order + [n - 1]:
        relay(step)
        for action in work.get(step, ()):
            action()
    front(last_tile)
    pair_sum_tile(far_tile)
    back(last_tile)
    pair_send_tile(last_tile)
    for tile in near_tiles[:-1]:
        pair_sum_tile(tile)
    back(near_tiles[-1])
    pair_send_tile(near_tiles[-1])
    begin(act_copy(my_b, 1))
    phase("j_wgrad0")
    lax.fori_loop(0, 2, up_step, 0)
    pair_sum_tile(last_tile)
    phase("j_wgrad1")
    lax.fori_loop(2, 5, up_step, 0)
    pair_sum_tile(near_tiles[-1])
    w_arrival(flipped(my_z, nz // 2))
    for part in range(1, nz // 2):
        begin(w_copy(flipped(my_z, nz // 2), part))
    phase("j_wgrad3")
    lax.fori_loop(5, steps_up, up_step, 0)
    act_arrival(flipped(my_b, 1))
    for part in range(2, q, 2):
        begin(act_copy(flipped(my_b, 1), part))
    phase("j_wgrad2")
    lax.fori_loop(0, steps_down, down_step, 0)
    phase("k_final_wait")
    for step in range(2, n, 2):
        index = lax.div(flipped(me, step), 2)
        remote(
            half.at[0], final.at[index], fin_send.at[0], fin_recv.at[index], (beside, core)
        ).wait_recv()

    phase("l_gs")
    gs_total = contract(final[...].reshape(experts * cap, width), flat_table, 0, 0)
    gs_total = gs_total + contract(grad_ref[...], identity(tok, BF16), 0, 0)
    gs_own[...] = gs_total.astype(BF16).reshape(gs_own.shape)

    part = pl.ds(core * (nz // 2), nz // 2)
    for step in range(1, q):
        peer = flipped(my_b, step)
        begin(
            remote(
                gs_own.at[:, peer],
                gs_all.at[my_b, part],
                gs_send.at[step, 0],
                gs_recv.at[my_b, core],
                (my_z * q + peer, core),
            )
        )
    gs_copy = pltpu.make_async_copy(gs_own.at[:, my_b], gs_all.at[my_b, part], local_sem.at[1])
    gs_copy.start()

    def gs_arrived(origin, source):
        remote(
            gs_own.at[:, 0],
            gs_all.at[origin, pl.ds(source * (nz // 2), nz // 2)],
            gs_send.at[0, 0],
            gs_recv.at[origin, source],
            (me, other),
        ).wait_recv()

    for step in range(q):
        origin = flipped(my_b, step)
        source = gs_own.at[:, my_b]
        if step:
            gs_arrived(origin, core)
            source = gs_all.at[origin, part]
        begin(
            remote(
                source,
                gs_all.at[origin, part],
                gs_send.at[step, 1],
                gs_recv.at[origin, core],
                (me, other),
            )
        )
    for step in range(1, nz):
        if step != nz // 2:
            w_arrival(flipped(my_z, step))
    for step in range(2, q):
        act_arrival(flipped(my_b, step))
    gs_copy.wait()
    for step in range(q):
        gs_arrived(flipped(my_b, step), other)

    phase("m_q")
    line_rows = nz * own_rows
    for b in range(q):
        product = jnp.dot(
            gs_all[b].reshape(line_rows, tok), act_all[b], preferred_element_type=F32
        ).reshape(nz, own_rows, width)
        q_sum[...] = product if b == 0 else q_sum[...] + product
    q_out[...] = q_sum[...].astype(BF16)
    for step in list(range(2, nz, 2)) + [0]:
        begin(
            remote(
                q_out.at[flipped(my_z, step + 1)],
                q_near.at[step // 2],
                q_send.at[step + 1],
                near_recv.at[step // 2],
                (flipped(me, q), core),
            )
        )

    def near_arrived(step):
        remote(
            q_out.at[0], q_near.at[step // 2], q_send.at[0], near_recv.at[step // 2], (beside, core)
        ).wait_recv()

    phase("n_p")
    w_line = w_all[...].reshape(line_rows, width)
    for step in range(1, q):
        target = lax.rem(my_b + step, q)
        p_out[target] = contract(gs_all[target].reshape(line_rows, tok), w_line, 0, 0).astype(BF16)
        copy = remote(
            p_out.at[target], p_in.at[my_b], p_send.at[step], p_recv.at[my_b], (in_square(step), core)
        )
        copy.start()
        sent.append(copy)
    p_own[...] = contract(gs_all[my_b].reshape(line_rows, tok), w_line, 0, 0)
    phase("n_q_on")
    for step in range(2, nz, 2):
        target = flipped(my_z, step)
        near_arrived(step)
        q_out[target] = (q_sum[target] + q_near[step // 2].astype(F32)).astype(BF16)
        begin(
            remote(
                q_out.at[target],
                q_in.at[my_z],
                q_send.at[step],
                q_recv.at[my_z],
                (flipped(me, step * q), core),
            )
        )
    phase("n_p_wait")
    for step in range(1, q):
        origin = lax.rem(my_b + step, q)
        remote(
            p_out.at[0], p_in.at[origin], p_send.at[0], p_recv.at[origin], (beside, core)
        ).wait_recv()

    phase("o_gn")
    def gn_step(i, carry):
        at = pl.ds(pl.multiple_of(i * chunk, chunk), chunk)
        grad_act = p_own[at, :]
        for step in range(1, q):
            grad_act = grad_act + p_in[lax.rem(my_b + step, q), at, :].astype(F32)
        normed = normed_of(at)
        z = normed * gain_ref[...]
        sig = jax.nn.sigmoid(z)
        gn = grad_act * sig * (1.0 + z * (1.0 - sig)) * gain_ref[...]
        gn_ref[at, :] = gn
        stat_out[0, at, :] = jnp.broadcast_to(jnp.sum(gn, axis=1, keepdims=True), (chunk, 128))
        stat_out[1, at, :] = jnp.broadcast_to(
            jnp.sum(gn * normed, axis=1, keepdims=True), (chunk, 128)
        )
        return carry

    lax.fori_loop(0, tok // chunk, gn_step, 0)
    stat2_copy = remote(stat_out, stat_in, stat_sem.at[2], stat_sem.at[3], (me, other))
    stat2_copy.start()
    stat2_copy.wait()

    phase("p_gc_halo")

    def conv_grad_step(i, carry):
        at = pl.ds(pl.multiple_of(i * chunk, chunk), chunk)
        first_mean = (stat_out[0, at, :] + stat_in[0, at, :])[:, 0:1] / depth
        second_mean = (stat_out[1, at, :] + stat_in[1, at, :])[:, 0:1] / depth
        grad_conv = inv_ref[at, 0:1] * (gn_ref[at, :] - first_mean - normed_of(at) * second_mean)
        ext_ref[at, :] = grad_conv.astype(BF16)
        return carry

    reach = ext_ref.shape[0] - tok
    previous = lax.rem(me + n - 1, n)
    halo = remote(
        ext_ref.at[pl.ds(0, reach)],
        ext_ref.at[pl.ds(tok, reach)],
        halo_sem.at[0],
        halo_sem.at[1],
        (previous, core),
    )
    lax.fori_loop(0, reach // chunk, conv_grad_step, 0)
    halo.start()
    lax.fori_loop(reach // chunk, tok // chunk, conv_grad_step, 0)

    out_ext[0:tok, :] = ext_ref[0:tok, :]
    phase("r_qwait")
    near_arrived(0)
    for step in range(2, nz, 2):
        origin = flipped(my_z, step)
        remote(
            q_out.at[0], q_in.at[origin], q_send.at[0], q_recv.at[origin], (beside, core)
        ).wait_recv()
    phase("r_halo_wait")
    halo.wait()
    after_rows = ext_ref[tok : tok + reach, :].astype(F32)
    out_ext[tok : tok + reach, :] = jnp.where(me == n - 1, 0.0, after_rows).astype(BF16)
    proj_total = q_sum[my_z] + q_near[0].astype(F32)
    for step in range(2, nz, 2):
        proj_total = proj_total + q_in[flipped(my_z, step)].astype(F32)
    out_proj[...] = proj_total

    phase("s_end")
    for step in range(steps_up - 2, steps_up):
        for copy in up_copies(step, step % 2):
            copy.wait()
    for step in range(steps_down - 2, steps_down):
        down_copy(step, step % 2).wait()
    for copy in sent:
        copy.wait_send()
    phase(None)


def finish_kernel(
    ext_hbm,
    taps_hbm,
    proj_hbm,
    gate_hbm,
    up_hbm,
    down_hbm,
    out_input,
    out_proj,
    out_gate,
    out_up,
    out_down,
    gate,
    up,
    down,
    ext,
    taps,
    proj,
    ext_f32,
    taps_f32,
    in_sem,
    out_sem,
    small_sem,
):
    small = [
        pltpu.make_async_copy(source, held, small_sem.at[i])
        for i, (source, held) in enumerate(((ext_hbm, ext), (taps_hbm, taps), (proj_hbm, proj)))
    ]
    for copy in small:
        copy.start()
    ins, outs = [], []
    for part in range(CHUNKS):
        for i, (source, held, result) in enumerate(
            ((gate_hbm, gate, out_gate), (up_hbm, up, out_up), (down_hbm, down, out_down))
        ):
            size = held.shape[0] // CHUNKS
            at = pl.ds(part * size, size)
            ins.append(pltpu.make_async_copy(source.at[0, at], held.at[at], in_sem.at[i, part]))
            outs.append(pltpu.make_async_copy(held.at[at], result.at[0, at], out_sem.at[i, part]))
    for copy in ins:
        copy.start()
    for copy in small:
        copy.wait()
    proj_copy = pltpu.make_async_copy(proj, out_proj, small_sem.at[3])
    proj_copy.start()
    taps_f32[...] = taps[...].astype(F32)
    tok, width = out_input.shape

    def conv_step(i, carry):
        lanes = pl.ds(pl.multiple_of(i * 128, 128), 128)
        ext_f32[:, lanes] = ext[:, lanes].astype(F32)
        total = jnp.zeros((tok, 128), F32)
        for k in range(taps.shape[0]):
            total = total + taps_f32[k : k + 1, lanes] * ext_f32[k : k + tok, lanes]
        out_input[:, lanes] = total.astype(BF16)
        return carry

    tiles = width // 128
    for part in range(CHUNKS):
        lax.fori_loop(part * tiles // CHUNKS, (part + 1) * tiles // CHUNKS, conv_step, 0)
        for copy_in, copy_out in zip(ins[3 * part : 3 * part + 3], outs[3 * part : 3 * part + 3]):
            copy_in.wait()
            copy_out.start()
    for copy in outs:
        copy.wait()
    proj_copy.wait()


def on_device(
    conv_out,
    ln_gain,
    taps,
    proj_weight,
    stream_mid,
    out_grad,
    routes,
    route_probs,
    gate_slabs,
    up_slabs,
    down_slabs,
):
    n = lax.axis_size("sp")
    q = 1
    while q * q * 4 <= n:
        q *= 2
    nz = n // q
    tok, width = conv_out.shape
    experts = n // 2
    cap = -(-(3 * tok // experts) // 16) * 16
    own_rows = proj_weight.shape[0]
    hidden = gate_slabs.shape[2]
    slots = n * cap
    reach = -(-(taps.shape[0] - 1) // 16) * 16
    vmem, dma = pltpu.VMEM, pltpu.SemaphoreType.DMA
    near = pl.BlockSpec(memory_space=pltpu.VMEM)
    far = pl.BlockSpec(memory_space=pl.ANY)
    buffers = [
        vmem(gate_slabs.shape[1:], BF16),
        vmem(up_slabs.shape[1:], BF16),
        vmem(down_slabs.shape[1:], BF16),
        vmem((experts, cap, tok), BF16),
        vmem((experts, 2, cap, width), BF16),
        vmem((n, 2, cap, 2 * width), BF16),
        vmem((experts, 8, 128), F32),
        vmem((n, 8, 128), F32),
        vmem((experts, tok), F32),
        vmem((experts, tok), F32),
        vmem((n, cap, 128), F32),
        vmem((q * cap, hidden), F32),
        vmem((q * cap, hidden), F32),
        vmem((q * cap, hidden), F32),
        vmem((slots, hidden), BF16),
        vmem((slots, hidden), BF16),
        vmem((slots, hidden), BF16),
        vmem((nz, q, cap, width), BF16),
        vmem((nz, q, cap, width), BF16),
        vmem((n, cap, width), BF16),
        vmem((experts, cap, width), BF16),
        vmem((experts, cap, width), BF16),
        vmem((2, 2, 256, hidden), BF16),
        vmem((2, hidden, 512), BF16),
        vmem((2, tok, 128), F32),
        vmem((2, tok, 128), F32),
        vmem((tok, 128), F32),
        vmem((tok, 128), F32),
        vmem((q, tok, width), BF16),
        vmem((nz, own_rows, width), BF16),
        vmem((nz // 2, q, own_rows, tok), BF16),
        vmem((q, nz, own_rows, tok), BF16),
        vmem((q, tok, width), BF16),
        vmem((q, tok, width), BF16),
        vmem((tok, width), F32),
        vmem((nz, own_rows, width), F32),
        vmem((nz, own_rows, width), BF16),
        vmem((nz, own_rows, width), BF16),
        vmem((nz // 2, own_rows, width), BF16),
        vmem((tok, width), F32),
        vmem((tok + reach, width), BF16),
    ]
    semaphores = [
        dma((3,)),
        dma((2, n // 2)),
        dma((2, n)),
        dma((2, n // 2)),
        dma((2, n)),
        dma((2, n)),
        dma((n,)),
        dma((n,)),
        dma((4,)),
        dma((nz, 2)),
        dma((nz,)),
        dma((q, 2)),
        dma((q,)),
        dma((nz,)),
        dma((nz,)),
        dma((experts,)),
        dma((experts,)),
        dma((experts,)),
        dma((experts,)),
        dma((q, 2)),
        dma((q, 2)),
        dma((q,)),
        dma((q,)),
        dma((nz,)),
        dma((nz,)),
        dma((nz // 2,)),
        dma((2,)),
        dma((3, 2)),
        dma((2,)),
    ]
    ext, proj, gate, up, down = pl.pallas_call(
        functools.partial(layer_kernel, n, q),
        out_shape=(
            jax.ShapeDtypeStruct((tok + reach, width), BF16),
            jax.ShapeDtypeStruct((own_rows, width), F32),
            jax.ShapeDtypeStruct(gate_slabs.shape, BF16),
            jax.ShapeDtypeStruct(up_slabs.shape, BF16),
            jax.ShapeDtypeStruct(down_slabs.shape, BF16),
        ),
        in_specs=[near] * 7 + [far] * 3,
        out_specs=(near, near, far, far, far),
        scratch_shapes=buffers + semaphores,
        compiler_params=pltpu.CompilerParams(
            collective_id=0, has_side_effects=True, vmem_limit_bytes=VMEM_BYTES
        ),
        cost_estimate=pl.CostEstimate(
            flops=16 * slots * 2 * width * hidden, bytes_accessed=60_000_000, transcendentals=0
        ),
    )(
        conv_out,
        ln_gain[None],
        proj_weight,
        stream_mid,
        out_grad,
        routes.T,
        route_probs.T,
        gate_slabs,
        up_slabs,
        down_slabs,
    )
    whole = [pltpu.VMEM(x.shape[1:], BF16) for x in (gate, up, down)]
    return pl.pallas_call(
        finish_kernel,
        out_shape=(
            jax.ShapeDtypeStruct((tok, width), BF16),
            jax.ShapeDtypeStruct(proj.shape, F32),
            jax.ShapeDtypeStruct(gate.shape, BF16),
            jax.ShapeDtypeStruct(up.shape, BF16),
            jax.ShapeDtypeStruct(down.shape, BF16),
        ),
        in_specs=[far] * 6,
        out_specs=(near, far, far, far, far),
        scratch_shapes=whole
        + [
            vmem(ext.shape, BF16),
            vmem(taps.shape, BF16),
            vmem(proj.shape, F32),
            vmem(ext.shape, F32),
            vmem(taps.shape, F32),
            dma((3, CHUNKS)),
            dma((3, CHUNKS)),
            dma((4,)),
        ],
        compiler_params=pltpu.CompilerParams(vmem_limit_bytes=VMEM_BYTES),
        cost_estimate=pl.CostEstimate(
            flops=2 * taps.shape[0] * tok * width, bytes_accessed=22_000_000, transcendentals=0
        ),
    )(ext, taps, proj, gate, up, down)


def solution(mesh):
    return jax.shard_map(
        on_device,
        mesh=mesh,
        in_specs=(
            P("sp", "tp"),
            P("tp"),
            P(None, "tp"),
            P("sp", "tp"),
            P("sp", "tp"),
            P("sp", "tp"),
            P("sp", None),
            P("sp", None),
            P("sp", None, "tp"),
            P("sp", None, "tp"),
            P("sp", "tp", None),
        ),
        out_specs=(
            P("sp", "tp"),
            P("sp", "tp"),
            P("sp", None, "tp"),
            P("sp", None, "tp"),
            P("sp", "tp", None),
        ),
        check_vma=False,
    )
```

time: 156 us -> 126 us (0.81); the launches traced: 156 us -> 124 us
  Pallas kernels: 139 us -> 123 us
  local copies, waits for them, and re-layouts: 15.9 us -> 0 us
    pallas_call x1, Pallas kernels: 139 us -> 113 us  [on_device(): pl.pallas_call(functools.partial(layer_kernel, n, q), out_shape=(jax.Shap...]
    unnamed x11 -> x0, local copies, waits for them, and re-layouts: 15.9 us -> none
    pallas_call x0 -> x1, Pallas kernels: none -> 9.68 us  [on_device(): pl.pallas_call(finish_kernel, out_shape=(jax.ShapeDtypeStruct((tok, width...]
where the time goes in v1:
time: 126 us; the launch traced here: 124 us
  Pallas kernels  123 us (98%)
    pallas_call x1, Pallas kernels, on_device(): pl.pallas_call(functools.partial(layer_kernel, n, q), out_shape=(jax.Shap...  113 us
    pallas_call x1, Pallas kernels, on_device(): pl.pallas_call(finish_kernel, out_shape=(jax.ShapeDtypeStruct((tok, width...  9.68 us

profile of v1, /device:TPU:14, one launch (start us, length us, event | category | flops | bytes accessed | tf_op | source)
XLA Modules:
  0.0 123.6 jit_solution(14027263454729433947)
XLA Ops:
  0.6 113.1 %shard_map.146 = (bf16[160,1024]{1,0:T(8,128)(2,1)}, f32[128,1024]{1,0:T(8,128)}, bf16[1,2048,896]{2,1,0:T(8,128)(2,1)}, bf16[1,2048,896]{2,1,0:T(8,128)(2,1)}, bf16[1,896,2048]{2,1,0:T(8,128)(2,1)}) custom-call(bf16[128,1024]{1,0:T(8,128)(2,1)} %conv_ref.1, f32[1,1024]{1,0:T(1,128)} %bitcast.3, bf16[128,1024]{1,0:T(8,128)(2,1)} %proj_ref.1, ...), custom_call_target="tpu_custom_call" | custom-call | flops 22548578304 | bytes 60000000 | tf_op jit(solution)/shard_map/pallas_call | solution.py:956
  113.7 9.7 %shard_map.147 = (bf16[128,1024]{1,0:T(8,128)(2,1)}, f32[128,1024]{1,0:T(8,128)}, bf16[1,2048,896]{2,1,0:T(8,128)(2,1)}, bf16[1,2048,896]{2,1,0:T(8,128)(2,1)}, bf16[1,896,2048]{2,1,0:T(8,128)(2,1)}) custom-call(bf16[160,1024]{1,0:T(8,128)(2,1)} %get-tuple-element.10.ext_hbm, bf16[31,1024]{1,0:T(8,128)(2,1)} %taps_hbm.1, ...), custom_call_target="tpu_custom_call" | custom-call | flops 8126464 | bytes 22000000 | tf_op jit(solution)/shard_map/pallas_call | solution.py:987

commit v2 on v1

--- a/solution.py
+++ b/solution.py
@@ -315,6 +315,7 @@
         stat_copy.wait()
         lax.fori_loop(0, tok // chunk, act_step, 0)
         w_all[my_z] = proj_ref[...]
+        begin(act_copy(my_b, 1))
         for part in range(2, q, 2):
             begin(act_copy(my_b, part))
 
@@ -569,6 +570,9 @@
         relay(step)
         for action in work.get(step, ()):
             action()
+    act_arrival(flipped(my_b, 1))
+    for part in range(2, q, 2):
+        begin(act_copy(flipped(my_b, 1), part))
     front(last_tile)
     pair_sum_tile(far_tile)
     back(last_tile)
@@ -577,23 +581,15 @@
         pair_sum_tile(tile)
     back(near_tiles[-1])
     pair_send_tile(near_tiles[-1])
-    begin(act_copy(my_b, 1))
-    phase("j_wgrad0")
-    lax.fori_loop(0, 2, up_step, 0)
     pair_sum_tile(last_tile)
     phase("j_wgrad1")
-    lax.fori_loop(2, 5, up_step, 0)
+    lax.fori_loop(0, 5, up_step, 0)
     pair_sum_tile(near_tiles[-1])
     w_arrival(flipped(my_z, nz // 2))
     for part in range(1, nz // 2):
         begin(w_copy(flipped(my_z, nz // 2), part))
     phase("j_wgrad3")
     lax.fori_loop(5, steps_up, up_step, 0)
-    act_arrival(flipped(my_b, 1))
-    for part in range(2, q, 2):
-        begin(act_copy(flipped(my_b, 1), part))
-    phase("j_wgrad2")
-    lax.fori_loop(0, steps_down, down_step, 0)
     phase("k_final_wait")
     for step in range(2, n, 2):
         index = lax.div(flipped(me, step), 2)
@@ -620,6 +616,8 @@
         )
     gs_copy = pltpu.make_async_copy(gs_own.at[:, my_b], gs_all.at[my_b, part], local_sem.at[1])
     gs_copy.start()
+
+    phase("l_gs_wait")
 
     def gs_arrived(origin, source):
         remote(
@@ -662,21 +660,44 @@
         ).reshape(nz, own_rows, width)
         q_sum[...] = product if b == 0 else q_sum[...] + product
     q_out[...] = q_sum[...].astype(BF16)
+    halves = [slice(0, width // 2), slice(width // 2, width)]
     for step in list(range(2, nz, 2)) + [0]:
-        begin(
-            remote(
-                q_out.at[flipped(my_z, step + 1)],
-                q_near.at[step // 2],
-                q_send.at[step + 1],
-                near_recv.at[step // 2],
-                (flipped(me, q), core),
+        for i, columns in enumerate(halves):
+            begin(
+                remote(
+                    q_out.at[flipped(my_z, step + 1), :, columns],
+                    q_near.at[step // 2, :, columns],
+                    q_send.at[step + 1, i],
+                    near_recv.at[step // 2, i],
+                    (flipped(me, q), core),
+                )
             )
-        )
-
-    def near_arrived(step):
+
+    def near_arrived(step, i):
         remote(
-            q_out.at[0], q_near.at[step // 2], q_send.at[0], near_recv.at[step // 2], (beside, core)
+            q_out.at[0, :, halves[i]],
+            q_near.at[step // 2, :, halves[i]],
+            q_send.at[0, 0],
+            near_recv.at[step // 2, i],
+            (beside, core),
         ).wait_recv()
+
+    def pass_on(i):
+        columns = halves[i]
+        for step in range(2, nz, 2):
+            target = flipped(my_z, step)
+            near_arrived(step, i)
+            total = q_sum[target, :, columns] + q_near[step // 2, :, columns].astype(F32)
+            q_out[target, :, columns] = total.astype(BF16)
+            begin(
+                remote(
+                    q_out.at[target, :, columns],
+                    q_in.at[my_z, :, columns],
+                    q_send.at[step, i],
+                    q_recv.at[my_z, i],
+                    (flipped(me, step * q), core),
+                )
+            )
 
     phase("n_p")
     w_line = w_all[...].reshape(line_rows, width)
@@ -689,20 +710,15 @@
         copy.start()
         sent.append(copy)
     p_own[...] = contract(gs_all[my_b].reshape(line_rows, tok), w_line, 0, 0)
-    phase("n_q_on")
-    for step in range(2, nz, 2):
-        target = flipped(my_z, step)
-        near_arrived(step)
-        q_out[target] = (q_sum[target] + q_near[step // 2].astype(F32)).astype(BF16)
-        begin(
-            remote(
-                q_out.at[target],
-                q_in.at[my_z],
-                q_send.at[step],
-                q_recv.at[my_z],
-                (flipped(me, step * q), core),
-            )
-        )
+    phase("n_wgrad")
+    lax.fori_loop(0, 1, down_step, 0)
+    phase("n_q_on0")
+    pass_on(0)
+    phase("n_q_on1")
+    lax.fori_loop(1, 2, down_step, 0)
+    pass_on(1)
+    phase("n_wgrad2")
+    lax.fori_loop(2, steps_down, down_step, 0)
     phase("n_p_wait")
     for step in range(1, q):
         origin = lax.rem(my_b + step, q)
@@ -757,12 +773,17 @@
 
     out_ext[0:tok, :] = ext_ref[0:tok, :]
     phase("r_qwait")
-    near_arrived(0)
-    for step in range(2, nz, 2):
-        origin = flipped(my_z, step)
-        remote(
-            q_out.at[0], q_in.at[origin], q_send.at[0], q_recv.at[origin], (beside, core)
-        ).wait_recv()
+    for i, columns in enumerate(halves):
+        near_arrived(0, i)
+        for step in range(2, nz, 2):
+            origin = flipped(my_z, step)
+            remote(
+                q_out.at[0, :, columns],
+                q_in.at[origin, :, columns],
+                q_send.at[0, 0],
+                q_recv.at[origin, i],
+                (beside, core),
+            ).wait_recv()
     phase("r_halo_wait")
     halo.wait()
     after_rows = ext_ref[tok : tok + reach, :].astype(F32)
@@ -946,9 +967,9 @@
         dma((q, 2)),
         dma((q,)),
         dma((q,)),
-        dma((nz,)),
-        dma((nz,)),
-        dma((nz // 2,)),
+        dma((nz, 2)),
+        dma((nz, 2)),
+        dma((nz // 2, 2)),
         dma((2,)),
         dma((3, 2)),
         dma((2,)),

time: 126 us -> 121 us (0.960); the launches traced: 124 us -> 120 us
  Pallas kernels: 123 us -> 119 us
    pallas_call x1, Pallas kernels: 113 us -> 109 us  [on_device(): pl.pallas_call(functools.partial(layer_kernel, n, q), out_shape=(jax.Shap...]
where the time goes in v2:
time: 121 us; the launch traced here: 120 us
  Pallas kernels  119 us (98%)
    pallas_call x1, Pallas kernels, on_device(): pl.pallas_call(functools.partial(layer_kernel, n, q), out_shape=(jax.Shap...  109 us
    pallas_call x1, Pallas kernels, on_device(): pl.pallas_call(finish_kernel, out_shape=(jax.ShapeDtypeStruct((tok, width...  9.68 us

profile of v2, /device:TPU:14, one launch (start us, length us, event | category | flops | bytes accessed | tf_op | source)
XLA Modules:
  0.0 119.9 jit_solution(17249239577307197024)
XLA Ops:
  0.6 109.4 %shard_map.146 = (bf16[160,1024]{1,0:T(8,128)(2,1)}, f32[128,1024]{1,0:T(8,128)}, bf16[1,2048,896]{2,1,0:T(8,128)(2,1)}, bf16[1,2048,896]{2,1,0:T(8,128)(2,1)}, bf16[1,896,2048]{2,1,0:T(8,128)(2,1)}) custom-call(bf16[128,1024]{1,0:T(8,128)(2,1)} %conv_ref.1, f32[1,1024]{1,0:T(1,128)} %bitcast.3, bf16[128,1024]{1,0:T(8,128)(2,1)} %proj_ref.1, ...), custom_call_target="tpu_custom_call" | custom-call | flops 22548578304 | bytes 60000000 | tf_op jit(solution)/shard_map/pallas_call | solution.py:977
  110.1 9.7 %shard_map.147 = (bf16[128,1024]{1,0:T(8,128)(2,1)}, f32[128,1024]{1,0:T(8,128)}, bf16[1,2048,896]{2,1,0:T(8,128)(2,1)}, bf16[1,2048,896]{2,1,0:T(8,128)(2,1)}, bf16[1,896,2048]{2,1,0:T(8,128)(2,1)}) custom-call(bf16[160,1024]{1,0:T(8,128)(2,1)} %get-tuple-element.10.ext_hbm, bf16[31,1024]{1,0:T(8,128)(2,1)} %taps_hbm.1, ...), custom_call_target="tpu_custom_call" | custom-call | flops 8126464 | bytes 22000000 | tf_op jit(solution)/shard_map/pallas_call | solution.py:1008
